TPU v7x, 768 devices: a whole 4x8x12 slice. The times are simulated.
768 devices in a mesh: rep: 3 (over z_hi), fs: 32 (over z_lo, y), tp: 8 (over x, core).
Axes of the slice: x: 4, y: 8, z: 12 (z_hi: 3, z_lo: 4; z = z_hi * 4 + z_lo), core: 2. Of those that a mesh axis runs over, the one named last changes fastest.
Arguments:
- tokens: bfloat16 [96, 512, 2048], P(('rep', 'fs')), may hold values from -6 to 6
- first_gain: float32 [2048], replicated, may hold values from 0.1 to 1.9
- in_matrix: float32 [2048, 2048], P('fs', 'tp'), may hold values from -0.125 to 0.125
- in_scale: float32 [2048], P('tp'), may hold values from 0.5 to 2
- conv_taps: float32 [4, 2048], P(None, 'tp'), may hold values from -3 to 3
- decay_rate: float32 [2, 2048], P(None, 'tp'), may hold values from 0 to 1, as said below
- recall_maps: float32 [2, 8, 256, 256], P(None, 'tp'), may hold values from -0.375 to 0.375
- admit_maps: float32 [2, 8, 256, 256], P(None, 'tp'), may hold values from -0.375 to 0.375
- out_matrix: float32 [2048, 2048], P('fs', 'tp'), may hold values from -0.125 to 0.125
- out_scale: float32 [2048], P('fs'), may hold values from 0.5 to 2
- second_gain: float32 [2048], replicated, may hold values from 0.1 to 1.9
- up_matrix: float32 [2048, 4096], P('fs', 'tp'), may hold values from -0.125 to 0.125
- up_scale: float32 [4096], P('tp'), may hold values from 0.5 to 2
- down_matrix: float32 [2048, 4096], P('fs', 'tp'), may hold values from -0.09375 to 0.09375
- down_scale: float32 [2048], P('fs'), may hold values from 0.5 to 2
Outputs:
- layer_out: bfloat16 [96, 512, 2048], P(('rep', 'fs'))
Inputs may be any that keep to these rules, and one draw needn't show every extreme that they name: `decay_rate`: positive per-step decay rates.
All inputs are finite; a program needn't handle non-finite values.
Results may differ from a plain program's by a relative error of at most 0.024.
Values may be sent and summed in bfloat16 or wider, within the bound.
A program may use at most 64 MiB of HBM per device.

v0:
```python
import math

import jax
import jax.numpy as jnp
from jax import lax
from jax.sharding import PartitionSpec as P

EPSILON = 1e-06
RATE_GAIN = 8.0


def sent_together(arrays, axis, dim, along):
    widths = [math.prod(a.shape[along:]) for a in arrays]
    both = jnp.concatenate(
        [a.reshape(*a.shape[:along], w) for a, w in zip(arrays, widths)], axis=along
    )
    out = lax.all_gather(both, axis, axis=dim, tiled=True)
    pieces = jnp.split(out, [sum(widths[:k]) for k in range(1, len(widths))], axis=along)
    return tuple((b.reshape(*out.shape[:along], *a.shape[along:]) for a, b in zip(arrays, pieces)))


def in_one_piece(arrays, axis, dim, along):
    widths = [a.shape[along] for a in arrays]
    both = jnp.concatenate(arrays, axis=along)
    out = lax.all_gather(both, axis, axis=dim, tiled=True)
    return tuple(jnp.split(out, [sum(widths[:k]) for k in range(1, len(widths))], axis=along))


def cut_along(value, dim, peers):
    before, after = (value.shape[:dim], value.shape[dim + 1 :])
    return jnp.moveaxis(value.reshape(*before, peers, -1, *after), dim, 0)


def sum_at_owner(value, axis, dim):
    pieces = cut_along(value, dim, lax.axis_size(axis))
    arrived = lax.all_to_all(pieces, axis, split_axis=0, concat_axis=0, tiled=True)
    return arrived.astype(jnp.float32).sum(axis=0)


def joined_along(pieces, dim):
    pieces = jnp.moveaxis(pieces, 0, dim)
    lengths = pieces.shape
    return pieces.reshape(*lengths[:dim], lengths[dim] * lengths[dim + 1], *lengths[dim + 2 :])


def from_everyone(value, axis):
    copies = jnp.broadcast_to(value, (lax.axis_size(axis), *value.shape))
    return lax.all_to_all(copies, axis, split_axis=0, concat_axis=0, tiled=True)


def collect(value, axis, dim):
    return joined_along(from_everyone(value, axis), dim)


def normalize(stream, gain):
    return stream * lax.rsqrt(jnp.mean(stream * stream, axis=-1, keepdims=True) + EPSILON) * gain


def convolve(values, taps):
    length = values.shape[0]
    count = taps.shape[0]
    padded = jnp.pad(values, ((count // 2, count - 1 - count // 2), (0, 0)))
    total = taps[0] * padded[0:length]
    for offset in range(1, count):
        total = total + taps[offset] * padded[offset : offset + length]
    return total


def block_map(values, maps):
    length = values.shape[0]
    count, width = (maps.shape[0], maps.shape[1])
    grouped = values.reshape(length, count, width)
    mapped = jnp.einsum("lnj,njk->lnk", grouped, maps)
    return mapped.reshape(length, count * width)


def combine_steps(earlier, later):
    return (earlier[0] * later[0], later[0] * earlier[1] + later[1])


def one_direction(values, rate, recall_map, admit_map):
    recall = jax.nn.sigmoid(block_map(values, recall_map))
    admit = jax.nn.sigmoid(block_map(values, admit_map))
    log_decay = -RATE_GAIN * recall * rate
    decay = jnp.exp(log_decay)
    drive = jnp.sqrt(-jnp.expm1(2.0 * log_decay)) * admit * values
    carried = lax.associative_scan(combine_steps, (decay, drive), axis=0)
    return carried[1]


def recurrence(values, rates, recall_maps, admit_maps):
    forward = one_direction(values, rates[0], recall_maps[0], admit_maps[0])
    backward = one_direction(values[::-1], rates[1], recall_maps[1], admit_maps[1])[::-1]
    return forward + backward


def contract_last(left, right):
    return lax.dot_general(
        left, right, (((1,), (1,)), ((), ())), preferred_element_type=jnp.float32
    )


def body(
    tokens,
    first_gain,
    in_matrix,
    in_scale,
    conv_taps,
    decay_rate,
    recall_maps,
    admit_maps,
    out_matrix,
    out_scale,
    second_gain,
    up_matrix,
    up_scale,
    down_matrix,
    down_scale,
):
    stream = tokens.reshape(tokens.shape[1], tokens.shape[2]).astype(jnp.float32)
    in_cols, out_rows, out_factor, down_factor = sent_together(
        (
            in_matrix.astype(jnp.bfloat16),
            out_matrix.astype(jnp.bfloat16),
            out_scale.astype(jnp.bfloat16),
            down_scale.astype(jnp.bfloat16),
        ),
        "fs",
        0,
        1,
    )
    up_cols, down_rows = in_one_piece(
        (up_matrix.astype(jnp.bfloat16), down_matrix.astype(jnp.bfloat16)), "fs", 0, 1
    )
    normed = normalize(stream, first_gain).astype(jnp.bfloat16)
    before = (
        jnp.dot(normed, in_cols, preferred_element_type=jnp.float32) * in_scale.astype(jnp.bfloat16)
    ).astype(jnp.bfloat16)
    conv_out = convolve(before.astype(jnp.float32), conv_taps)
    mixed = recurrence(conv_out, decay_rate, recall_maps, admit_maps).astype(jnp.bfloat16)
    partial_value = contract_last(mixed, out_rows)
    share = stream.shape[0] // lax.axis_size("tp")
    own_start = lax.axis_index("tp") * share
    own_stream = lax.dynamic_slice_in_dim(stream, own_start, share, 0)
    middle = own_stream + out_factor * sum_at_owner(partial_value.astype(jnp.bfloat16), "tp", 0)
    own_normed = normalize(middle, second_gain).astype(jnp.bfloat16)
    second_normed = collect(own_normed, "tp", 0)
    raised = jnp.dot(second_normed, up_cols, preferred_element_type=jnp.float32)
    active = jnp.square(jax.nn.relu(raised * up_scale.astype(jnp.bfloat16))).astype(jnp.bfloat16)
    lowered = contract_last(active, down_rows)
    finished = (middle + down_factor * sum_at_owner(lowered.astype(jnp.bfloat16), "tp", 0)).astype(
        jnp.bfloat16
    )
    result = collect(finished, "tp", 0)
    return result.reshape(tokens.shape)


def solution(mesh):
    placed = (
        P(("rep", "fs"), None, None),
        P(),
        P("fs", "tp"),
        P("tp"),
        P(None, "tp"),
        P(None, "tp"),
        P(None, "tp", None, None),
        P(None, "tp", None, None),
        P("fs", "tp"),
        P("fs"),
        P(),
        P("fs", "tp"),
        P("tp"),
        P("fs", "tp"),
        P("fs"),
    )
    return jax.shard_map(
        body, mesh=mesh, in_specs=placed, out_specs=P(("rep", "fs"), None, None), check_vma=False
    )
```

profile of v0, /device:TPU:1, one launch (start us, length us, event | category | flops | bytes accessed | tf_op | source)
XLA Modules:
  0.0 501.1 jit_solution(15447023195010164814)
XLA Ops:
  14.1 2.1 fusion
  16.8 138.1 %all-gather.3.cloned.1.call-done = bf16[2048,514]{1,0:T(8,128)(2,1)} async-done(((bf16[64,514]{1,0:T(8,128)(2,1)}), bf16[2048,514]{1,0:T(8,128)(2,1)}) %all-gather.3.cloned.1.call-update) | async-done | bytes 2105360 | tf_op jit(solution)/shard_map/all_gather | solution.py:17
  155.0 2.0 fusion.47
  160.7 2.5 slice.466
  163.1 2.5 slice.470
  220.5 1.9 slice.530
  222.4 2.5 slice.465
  225.2 1.5 fusion.103
  226.8 1.9 fusion.40
  238.2 1.8 fusion.89
  241.2 1.5 slice.548
  242.8 1.5 slice.552
  244.3 1.6 fusion.91
  287.3 1.5 slice.547
  293.6 2.5 slice.535
  309.5 1.7 pad.131
  320.1 2.7 pad.150
  323.8 1.7 pad.149
  325.5 2.1 add.346
  327.5 4.8 rev.7
  332.3 3.5 convolution_convert_fusion
  335.8 26.7 %all-to-all-start = ((bf16[8,64,2048]{2,1,0:T(8,128)(2,1)}), bf16[8,64,2048]{2,1,0:T(8,128)(2,1)}, u32[]{:S(2)}, u32[]{:S(2)}) async-start(bf16[8,64,2048]{2,1,0:T(8,128)(2,1)} %bitcast.54), calls=%async_computation | async-start | bytes 4194304 | tf_op jit(solution)/shard_map/all_to_all | solution.py:36
  362.5 2.5 convert_element_type.91
  365.0 1.8 convert_reduce_fusion.2
  366.9 21.9 %all-to-all-done = bf16[8,64,2048]{2,1,0:T(8,128)(2,1)} async-done(((bf16[8,64,2048]{2,1,0:T(8,128)(2,1)}), bf16[8,64,2048]{2,1,0:T(8,128)(2,1)}, u32[]{:S(2)}, u32[]{:S(2)}) %all-to-all-start) | async-done | bytes 2097184 | tf_op jit(solution)/shard_map/all_to_all | solution.py:36
  388.8 2.0 convert_reduce_fusion.1
  392.2 1.6 broadcast_in_dim.4
  393.8 5.3 %all-to-all-start.1 = ((bf16[8,64,2048]{2,1,0:T(8,128)(2,1)}), bf16[8,64,2048]{2,1,0:T(8,128)(2,1)}, u32[]{:S(2)}, u32[]{:S(2)}) async-start(bf16[8,64,2048]{2,1,0:T(8,128)(2,1)} %broadcast_in_dim.4), calls=%async_computation.1 | async-start | bytes 4194304 | tf_op jit(solution)/shard_map/all_to_all | solution.py:48
  399.1 26.3 %all-to-all-done.1 = bf16[8,64,2048]{2,1,0:T(8,128)(2,1)} async-done(((bf16[8,64,2048]{2,1,0:T(8,128)(2,1)}), bf16[8,64,2048]{2,1,0:T(8,128)(2,1)}, u32[]{:S(2)}, u32[]{:S(2)}) %all-to-all-start.1) | async-done | bytes 2097184 | tf_op jit(solution)/shard_map/all_to_all | solution.py:48
  425.4 6.5 %convolution_convert_fusion.1 = bf16[512,2048]{1,0:T(8,128)(2,1)} fusion(bf16[2048,1024]{1,0:T(8,128)(2,1)} %all-gather.5.cloned.1.call-done, bf16[512,2048]{1,0:T(8,128)(2,1)} %bitcast.15, f32[512]{0:T(512)S(1)} %convert_convert_fusion), kind=kOutput, calls=%fused_computation.8 | convolution fusion | flops 2149580800 | bytes 8390656 | tf_op jit(solution)/shard_map/dot_general | solution.py:98
  432.0 30.6 %all_to_all.20 = bf16[8,64,2048]{2,1,0:T(8,128)(2,1)S(1)} all-to-all(bf16[8,64,2048]{2,1,0:T(8,128)(2,1)} %bitcast.56), channel_id=1, replica_groups=mesh['rep'=3,'fs'=32,'tp'=8] {'tp'}, dimensions={0} | all-to-all | bytes 4194304 | tf_op jit(solution)/shard_map/all_to_all | solution.py:36
  463.3 29.7 %all_to_all.21 = bf16[8,64,2048]{2,1,0:T(8,128)(2,1)S(1)} all-to-all(bf16[8,64,2048]{2,1,0:T(8,128)(2,1)S(1)} %broadcast_in_dim.5), channel_id=1, replica_groups=mesh['rep'=3,'fs'=32,'tp'=8] {'tp'}, dimensions={0} | all-to-all | bytes 4194304 | tf_op jit(solution)/shard_map/all_to_all | solution.py:48
  (274 shorter events, 150.0 us)
Async XLA Ops:
  6.5 148.4 %copy-start = (bf16[1,512,2048]{2,1,0:T(8,128)(2,1)S(1)}, bf16[1,512,2048]{2,1,0:T(8,128)(2,1)}, u32[]{:S(2)}) copy-start(bf16[1,512,2048]{2,1,0:T(8,128)(2,1)} %param.15) | copy-start | bytes 6291460
  6.5 9.7 %copy-start.19 = (f32[256]{0:T(256)S(1)}, f32[256]{0:T(256)}, u32[]{:S(2)}) copy-start(f32[256]{0:T(256)} %param.18) | copy-start | bytes 3076
  6.5 9.7 %copy-start.17 = (f32[2,256]{1,0:T(2,128)S(1)}, f32[2,256]{1,0:T(2,128)}, u32[]{:S(2)}) copy-start(f32[2,256]{1,0:T(2,128)} %param.20) | copy-start | bytes 6148
  6.5 148.4 %copy-start.24 = (f32[2048]{0:T(1024)S(1)}, f32[2048]{0:T(1024)}, u32[]{:S(2)}) copy-start(f32[2048]{0:T(1024)} %param.16) | copy-start | bytes 24580
  6.5 148.4 %all-gather.3.cloned.1.call-start = ((), (), s32[]{:S(2)}) async-start(), calls=%async_computation.4 | async-start | bytes 2703360 | tf_op jit(solution)/shard_map/all_gather | solution.py:17
  10.7 414.7 %all-gather.5.cloned.1.call-start = ((), (), s32[]{:S(2)}) async-start(), calls=%async_computation.5 | async-start | bytes 4325376 | tf_op jit(solution)/shard_map/all_gather | solution.py:25
  16.8 140.4 %copy-start.21 = (f32[2,1,256,256]{3,2,1,0:T(8,128)S(1)}, f32[2,1,256,256]{3,2,1,0:T(8,128)}, u32[]{:S(2)}) copy-start(f32[2,1,256,256]{3,2,1,0:T(8,128)} %param.21) | copy-start | bytes 1572868
  157.0 1.4 copy-start.22
  158.9 4.2 copy-start.2
  210.6 14.6 %copy-start.20 = (f32[1,256]{1,0:T(1,128)S(1)}, f32[1,256]{1,0:T(1,128)}, u32[]{:S(2)}) copy-start(f32[1,256]{1,0:T(1,128)} %get-tuple-element.48) | copy-start | bytes 3076
  225.2 1.6 copy-start.10
  225.2 1.6 copy-start.23
  226.7 6.1 %copy-start.4 = (f32[512,256]{1,0:T(8,128)}, f32[512,256]{1,0:T(8,128)S(1)}, u32[]{:S(2)}) copy-start(f32[512,256]{1,0:T(8,128)S(1)} %get-tuple-element.51) | copy-start | bytes 1572868
  228.7 67.5 %copy-start.3 = (f32[512,256]{1,0:T(8,128)}, f32[512,256]{1,0:T(8,128)S(1)}, u32[]{:S(2)}) copy-start(f32[512,256]{1,0:T(8,128)S(1)} %fusion.40) | copy-start | bytes 1572868
  271.0 33.9 %copy-start.14 = (f32[4,256]{1,0:T(4,128)}, f32[4,256]{1,0:T(4,128)S(1)}, u32[]{:S(2)}) copy-start(f32[4,256]{1,0:T(4,128)S(1)} %get-tuple-element.39) | copy-start | bytes 12292
  290.0 14.9 %copy-start.6 = (f32[127,256]{1,0:T(8,128)S(1)}, f32[127,256]{1,0:T(8,128)}, u32[]{:S(2)}) copy-start(f32[127,256]{1,0:T(8,128)} %slice.528) | copy-start | bytes 390148
  291.7 11.6 %copy-start.11 = (f32[63,256]{1,0:T(8,128)S(1)}, f32[63,256]{1,0:T(8,128)}, u32[]{:S(2)}) copy-start(f32[63,256]{1,0:T(8,128)} %slice.477) | copy-start | bytes 193540
  291.7 13.3 %copy-start.7 = (f32[127,256]{1,0:T(8,128)S(1)}, f32[127,256]{1,0:T(8,128)}, u32[]{:S(2)}) copy-start(f32[127,256]{1,0:T(8,128)} %slice.471) | copy-start | bytes 390148
  296.2 8.9 %copy-start.16 = (f32[1,256]{1,0:T(1,128)S(1)}, f32[1,256]{1,0:T(1,128)}, u32[]{:S(2)}) copy-start(f32[1,256]{1,0:T(1,128)} %slice.602) | copy-start | bytes 3076
  305.0 4.4 slice-start
  306.9 10.7 %copy-start.12 = (f32[63,256]{1,0:T(8,128)S(1)}, f32[63,256]{1,0:T(8,128)}, u32[]{:S(2)}) copy-start(f32[63,256]{1,0:T(8,128)} %slice.547) | copy-start | bytes 193540
  307.0 10.7 %copy-start.13 = (f32[63,256]{1,0:T(8,128)S(1)}, f32[63,256]{1,0:T(8,128)}, u32[]{:S(2)}) copy-start(f32[63,256]{1,0:T(8,128)} %slice.596) | copy-start | bytes 193540
  308.0 10.4 %copy-start.8 = (f32[127,256]{1,0:T(8,128)S(1)}, f32[127,256]{1,0:T(8,128)}, u32[]{:S(2)}) copy-start(f32[127,256]{1,0:T(8,128)} %slice.598) | copy-start | bytes 390148
  308.0 10.4 %copy-start.9 = (f32[127,256]{1,0:T(8,128)S(1)}, f32[127,256]{1,0:T(8,128)}, u32[]{:S(2)}) copy-start(f32[127,256]{1,0:T(8,128)} %slice.541) | copy-start | bytes 390148
  317.7 5.1 %copy-start.5 = (f32[255,256]{1,0:T(8,128)S(1)}, f32[255,256]{1,0:T(8,128)}, u32[]{:S(2)}) copy-start(f32[255,256]{1,0:T(8,128)} %slice.600) | copy-start | bytes 783364
  318.5 5.3 %slice-start.1 = ((f32[512,256]{1,0:T(8,128)}), f32[1,256]{1,0:T(1,128)S(1)}, s32[]{:S(2)}) async-start(f32[512,256]{1,0:T(8,128)} %copy-done.3), calls=%async_computation.7 | async-start | bytes 2048 | tf_op jit(solution)/shard_map/slice | solution.py:87
  323.8 8.5 %copy-start.1 = (f32[512,256]{1,0:T(8,128)S(1)}, f32[512,256]{1,0:T(8,128)}, u32[]{:S(2)}) copy-start(f32[512,256]{1,0:T(8,128)} %pad.131) | copy-start | bytes 1572868
  335.8 53.0 %all-to-all-start = ((bf16[8,64,2048]{2,1,0:T(8,128)(2,1)}), bf16[8,64,2048]{2,1,0:T(8,128)(2,1)}, u32[]{:S(2)}, u32[]{:S(2)}) async-start(bf16[8,64,2048]{2,1,0:T(8,128)(2,1)} %bitcast.54), calls=%async_computation | async-start | bytes 4194304 | tf_op jit(solution)/shard_map/all_to_all | solution.py:36
  366.9 25.2 %copy-start.15 = (f32[2048]{0:T(1024)S(1)}, f32[2048]{0:T(1024)}, u32[]{:S(2)}) copy-start(f32[2048]{0:T(1024)} %param.25) | copy-start | bytes 24580
  393.8 5.3 %copy-start.18 = (f32[512]{0:T(512)S(1)}, f32[512]{0:T(512)}, u32[]{:S(2)}) copy-start(f32[512]{0:T(512)} %param.27) | copy-start | bytes 6148
  393.8 31.7 %all-to-all-start.1 = ((bf16[8,64,2048]{2,1,0:T(8,128)(2,1)}), bf16[8,64,2048]{2,1,0:T(8,128)(2,1)}, u32[]{:S(2)}, u32[]{:S(2)}) async-start(bf16[8,64,2048]{2,1,0:T(8,128)(2,1)} %broadcast_in_dim.4), calls=%async_computation.1 | async-start | bytes 4194304 | tf_op jit(solution)/shard_map/all_to_all | solution.py:48
Sparse Core Ops, SparseCore 0:
  10.8 144.0 all-gather.2
  157.3 160.2 all-gather.4
where the time goes:
time: 506 us; the launch traced here: 501 us
  waiting for transfers between devices  186 us (37%)
  local copies, waits for them, and re-layouts  129 us (25%)
  other arithmetic  61.6 us (12%)
  blocking collectives  60.3 us (12%)
  starting transfers between devices  32.1 us (6%)
  matrix products  17.1 us (3%)
  between operations  14.1 us (3%)
    all_gather x1, waiting for transfers between devices, sent_together(): out = lax.all_gather(both, axis, axis=dim, tiled=True)  138 us
    slice x108, local copies, waits for them, and re-layouts, one_direction(): carried = lax.associative_scan(combine_steps, (decay, drive), axis=0)  112 us
    all_to_all x1, blocking collectives, sum_at_owner(): lax.all_to_all(pieces, axis, split_axis=0, concat_axis=0, tiled=True)  30.6 us
    all_to_all x1, blocking collectives, from_everyone(): return lax.all_to_all(copies, axis, split_axis=0, concat_axis=0, tiled=True)  29.7 us
    all_to_all x1, starting transfers between devices, sum_at_owner(): lax.all_to_all(pieces, axis, split_axis=0, concat_axis=0, tiled=True)  26.7 us
    all_to_all x1, waiting for transfers between devices, from_everyone(): return lax.all_to_all(copies, axis, split_axis=0, concat_axis=0, tiled=True)  26.3 us
    all_to_all x1, waiting for transfers between devices, sum_at_owner(): lax.all_to_all(pieces, axis, split_axis=0, concat_axis=0, tiled=True)  21.9 us
    mul x14, other arithmetic, combine_steps(): return (earlier[0] * later[0], later[0] * earlier[1] + later[1])  18.1 us
  transfers between devices with their start and end apart: 4, of which 3 were waited for; matrix products, arithmetic and copies ran while one was open for 39% of the time, Pallas kernels for 0%

commit v1 on v0

v1 whole, which is shorter than its diff:
```python
import functools

import jax
import jax.numpy as jnp
from jax import lax
from jax.experimental import pallas as pl
from jax.experimental.pallas import tpu as pltpu
from jax.sharding import PartitionSpec as P

EPSILON = 1e-06
RATE_GAIN = 8.0
MESH = pl.DeviceIdType.MESH
F32, BF16 = jnp.float32, jnp.bfloat16
NZ, NY, NX = 4, 8, 4
CHUNK, CHUNKS = 64, 8
PAD = 8
COPIES = 120


def nt_dot(left, right):
    return lax.dot_general(left, right, (((1,), (1,)), ((), ())), preferred_element_type=F32)


def as_column(row):
    n = row.shape[1]
    eye = lax.broadcasted_iota(jnp.int32, (n, n), 0) == lax.broadcasted_iota(jnp.int32, (n, n), 1)
    return jnp.sum(jnp.where(eye, jnp.broadcast_to(row, (n, n)), 0.0), axis=1, keepdims=True)


def rounded(value):
    return value.astype(BF16).astype(F32)


def kernel(
    tokens, first_gain, in_matrix, in_scale, conv_taps, decay_rate, recall_maps, admit_maps,
    out_matrix, out_scale, second_gain, up_matrix, up_scale, down_matrix, down_scale,
    result,
    in_all, out_all, up_all, down_all, normed, padded, conv, recall, admit, state, gain, mixed,
    part, paired, sums, relay_a, relay_b, from_left, from_right, middle, second, active,
    part2, paired2, sums2, relay2_a, relay2_b, from_left2, from_right2,
    send_sem, recv_sem,
):
    r, f, t = lax.axis_index("rep"), lax.axis_index("fs"), lax.axis_index("tp")
    zl, y = f // NY, f % NY
    z, depth = r * NZ + zl, 3 * NZ
    x, c = t // 2, t % 2
    z_up, z_down = (z + 1) % depth, (z + depth - 1) % depth
    Y_UP, Y_DOWN = (r, zl * NY + (y + 1) % NY, t), (r, zl * NY + (y + NY - 1) % NY, t)
    Z_UP, Z_DOWN = (z_up // NZ, (z_up % NZ) * NY + y, t), (z_down // NZ, (z_down % NZ) * NY + y, t)
    X_UP, X_DOWN = (r, f, (t + 2) % 8), (r, f, (t + 6) % 8)
    TWIN = (r, f, t + 1 - 2 * c)

    barrier = pltpu.get_barrier_semaphore()
    for peer in (Y_UP, Y_DOWN, Z_UP, Z_DOWN, X_UP, X_DOWN, TWIN):
        pl.semaphore_signal(barrier, inc=1, device_id=peer, device_id_type=MESH)

    started = []

    def send(src, dst, peer):
        k = len(started)
        copy = pltpu.make_async_remote_copy(
            src_ref=src, dst_ref=dst, send_sem=send_sem.at[k], recv_sem=recv_sem.at[k],
            device_id=peer, device_id_type=MESH,
        )
        copy.start()
        started.append(copy)
        return copy

    class Gather:
        def __init__(self, buf, split):
            self.buf, self.split, self.rows, self.waiting = buf, split, buf.shape[2], []
            self.step = 0

        def both(self, up, src_up, down, src_down):
            self.waiting.append(send(src_up, src_up, up))
            self.waiting.append(send(src_down, src_down, down))

        def go(self):
            for copy in self.waiting:
                copy.wait_recv()
            self.waiting = []
            buf, k = self.buf, self.step
            self.step += 1
            if self.split > 0:
                lo, mid, hi = 0, self.split // 2, self.split
                if k == 0:
                    own = buf.at[zl, y, lo:hi]
                    self.both(Z_UP, own, Z_DOWN, own)
                elif k == 1:
                    self.both(Z_UP, buf.at[(zl + 3) % NZ, y, lo:mid], Z_DOWN, buf.at[(zl + 1) % NZ, y, mid:hi])
                elif k in (2, 3, 4):
                    d = k - 2
                    self.both(Y_UP, buf.at[:, (y + NY - d) % NY, lo:hi], Y_DOWN, buf.at[:, (y + d) % NY, lo:hi])
                elif k == 5:
                    self.both(Y_UP, buf.at[:, (y + NY - 3) % NY, lo:mid], Y_DOWN, buf.at[:, (y + 3) % NY, mid:hi])
            if self.split < self.rows:
                lo, hi = self.split, self.rows
                mid = (lo + hi) // 2
                if k in (0, 1, 2):
                    self.both(Y_UP, buf.at[zl, (y + NY - k) % NY, lo:hi], Y_DOWN, buf.at[zl, (y + k) % NY, lo:hi])
                elif k == 3:
                    self.both(Y_UP, buf.at[zl, (y + NY - 3) % NY, lo:mid], Y_DOWN, buf.at[zl, (y + 3) % NY, mid:hi])
                elif k == 4:
                    own = buf.at[zl, :, lo:hi]
                    self.both(Z_UP, own, Z_DOWN, own)
                elif k == 5:
                    self.both(Z_UP, buf.at[(zl + 3) % NZ, :, lo:mid], Z_DOWN, buf.at[(zl + 1) % NZ, :, mid:hi])

    in_all[zl, y] = in_matrix[...].astype(BF16)
    out_all[zl, y] = (rounded(out_matrix[...]) * as_column(rounded(out_scale[...]))).astype(BF16)
    pl.semaphore_wait(barrier, 7)
    g_in, g_out = Gather(in_all, 32), Gather(out_all, 32)
    g_up, g_down = Gather(up_all, 64), Gather(down_all, 0)
    g_in.go()
    g_out.go()
    up_all[zl, y] = up_matrix[...].astype(BF16)
    down_all[zl, y] = (rounded(down_matrix[...]) * as_column(rounded(down_scale[...]))).astype(BF16)

    def normalize_rows(first, count):
        def step(i, carry):
            rows = pl.ds(pl.multiple_of(first + i * 32, 32), 32)
            value = tokens[0, rows, :].astype(F32)
            scale = lax.rsqrt(jnp.mean(value * value, axis=-1, keepdims=True) + EPSILON)
            normed[rows, :] = (value * scale * first_gain[...]).astype(BF16)
            return carry

        lax.fori_loop(0, count // 32, step, 0)

    for k in range(4):
        normalize_rows(128 * k, 128)
        g_in.go()
        g_out.go()
    padded[:, 0:PAD, :] = jnp.zeros((2, PAD, 128), F32)
    padded[:, PAD + 512 :, :] = jnp.zeros((2, PAD, 128), F32)
    g_in.go()
    g_out.go()
    g_in.go()
    g_out.go()
    g_down.go()
    g_up.go()

    def project(i, carry):
        rows = pl.ds(pl.multiple_of(i * 256, 256), 256)
        value = jnp.dot(normed[rows, :], in_all[...].reshape(2048, 256), preferred_element_type=F32)
        value = rounded(value * rounded(in_scale[...]))
        there = pl.ds(pl.multiple_of(PAD + i * 256, 8), 256)
        padded[0, there, :] = value[:, 0:128]
        padded[1, there, :] = value[:, 128:256]
        return carry

    lax.fori_loop(0, 2, project, 0)
    g_down.go()
    g_up.go()

    for half in range(2):
        lanes = pl.ds(half * 128, 128)
        taps = [conv_taps[k : k + 1, half * 128 : half * 128 + 128] for k in range(4)]

        def convolve(i, window):
            ahead = padded[half, pl.ds(i + PAD + 1, CHUNKS, stride=CHUNK), :]
            window = (*window, ahead)
            total = taps[0] * window[0] + taps[1] * window[1] + taps[2] * window[2] + taps[3] * window[3]
            conv[pl.ds(pl.multiple_of(i * 8, 8), 8), lanes] = total
            return window[1:]

        head = tuple(padded[half, pl.ds(PAD - 2 + k, CHUNKS, stride=CHUNK), :] for k in range(3))
        lax.fori_loop(0, CHUNK, convolve, head, unroll=4)

    g_down.go()
    g_up.go()
    values = conv[...].astype(BF16)
    for d in range(2):
        recall[d] = jnp.dot(values, recall_maps[d, 0].astype(BF16), preferred_element_type=F32)
        admit[d] = jnp.dot(values, admit_maps[d, 0].astype(BF16), preferred_element_type=F32)
    g_down.go()
    g_up.go()

    rates = [decay_rate[d : d + 1, :] * RATE_GAIN for d in range(2)]

    def scan_step(i, carry):
        new = []
        for d in range(2):
            h, g = carry[2 * d], carry[2 * d + 1]
            at = i if d == 0 else CHUNK - 1 - i
            rows = pl.ds(pl.multiple_of(at * 8, 8), 8)
            rate = 1.0 / (1.0 + jnp.exp(-recall[d, rows, :])) * rates[d]
            a = jnp.exp(-rate)
            u = jnp.tanh(rate)
            root = 2.0 * u * lax.rsqrt(jnp.maximum(2.0 * u * (1.0 + u), 1e-37))
            drive = root / (1.0 + jnp.exp(-admit[d, rows, :])) * conv[rows, :]
            h = a * h + drive
            g = a * g
            state[d, rows, :] = h
            gain[d, rows, :] = g
            new += [h, g]
        return tuple(new)

    zero, one = jnp.zeros((CHUNKS, 256), F32), jnp.ones((CHUNKS, 256), F32)
    ends = lax.fori_loop(0, CHUNK, scan_step, (zero, one, zero, one), unroll=4)

    def carried(h, g, order):
        row, rows = jnp.zeros((1, 256), F32), {}
        for s in order:
            rows[s] = row
            row = g[s : s + 1, :] * row + h[s : s + 1, :]
        return jnp.concatenate([rows[s] for s in range(CHUNKS)], axis=0)

    carry_0 = carried(ends[0], ends[1], range(CHUNKS))
    carry_1 = carried(ends[2], ends[3], range(CHUNKS - 1, -1, -1))

    def finish(i, carry):
        rows = pl.ds(pl.multiple_of(i * 8, 8), 8)
        total = state[0, rows, :] + gain[0, rows, :] * carry_0 + (state[1, rows, :] + gain[1, rows, :] * carry_1)
        mixed[0, pl.ds(i, CHUNKS, stride=CHUNK), :] = total[:, 0:128]
        mixed[1, pl.ds(i, CHUNKS, stride=CHUNK), :] = total[:, 128:256]
        return carry

    lax.fori_loop(0, CHUNK, finish, 0, unroll=4)
    g_down.go()
    g_up.go()

    x1, x2, x3 = (x + 1) % NX, (x + 2) % NX, (x + 3) % NX

    def summed_at_owner(left, weight, part, paired, sums, relay_a, relay_b, from_left, from_right, between):
        def tile(n, carry):
            w = weight[n // 2, pl.ds((n % 2) * 4, 4)]
            value = nt_dot(left, w.reshape(256, w.shape[-1])).astype(BF16)
            part[:, :, :, pl.ds(pl.multiple_of(n * 256, 256), 256)] = value.reshape(4, 2, 64, 256)
            return carry

        cols = (slice(0, 1024), slice(1024, 2048))
        twin = []
        for half in range(2):
            lax.fori_loop(4 * half, 4 * half + 4, tile, 0)
            twin.append(send(part.at[:, 1 - c, :, cols[half]], paired.at[:, :, cols[half]], TWIN))

        def pair_sum(owner, half):
            return part[owner, c, :, cols[half]].astype(F32) + paired[owner, :, cols[half]].astype(F32)

        twin[0].wait_recv()
        sums[2, :, cols[0]] = pair_sum(x2, 0).astype(BF16)
        relayed_a = send(sums.at[2, :, cols[0]], relay_a, X_DOWN)
        sums[1, :, cols[0]] = pair_sum(x1, 0).astype(BF16)
        left_a = send(sums.at[1, :, cols[0]], from_left.at[:, cols[0]], X_UP)
        twin[1].wait_recv()
        sums[2, :, cols[1]] = pair_sum(x2, 1).astype(BF16)
        relayed_b = send(sums.at[2, :, cols[1]], relay_b, X_UP)
        sums[3, :, cols[1]] = pair_sum(x3, 1).astype(BF16)
        right_b = send(sums.at[3, :, cols[1]], from_right.at[:, cols[1]], X_DOWN)
        relayed_a.wait_recv()
        sums[3, :, cols[0]] = (pair_sum(x3, 0) + relay_a[...].astype(F32)).astype(BF16)
        right_a = send(sums.at[3, :, cols[0]], from_right.at[:, cols[0]], X_DOWN)
        relayed_b.wait_recv()
        sums[1, :, cols[1]] = (pair_sum(x1, 1) + relay_b[...].astype(F32)).astype(BF16)
        left_b = send(sums.at[1, :, cols[1]], from_left.at[:, cols[1]], X_UP)
        between()
        for copy in (left_a, right_b, right_a, left_b):
            copy.wait_recv()
        own = part[x, c].astype(F32) + paired[x].astype(F32)
        return own + from_left[...].astype(F32) + from_right[...].astype(F32)

    def to_everyone(block):
        half_a, half_b = slice(0, 1024), slice(1024, 2048)
        below, above, across = (t + 6) % 8, (t + 2) % 8, (t + 4) % 8
        up = send(block(t), block(t), X_UP)
        down = send(block(t), block(t), X_DOWN)
        last = [send(block(t), block(t), TWIN)]
        up.wait_recv()
        over_a = send(block(below).at[:, half_a], block(below).at[:, half_a], X_UP)
        last.append(send(block(below), block(below), TWIN))
        down.wait_recv()
        over_b = send(block(above).at[:, half_b], block(above).at[:, half_b], X_DOWN)
        last.append(send(block(above), block(above), TWIN))
        over_a.wait_recv()
        last.append(send(block(across).at[:, half_a], block(across).at[:, half_a], TWIN))
        over_b.wait_recv()
        last.append(send(block(across).at[:, half_b], block(across).at[:, half_b], TWIN))
        for copy in last:
            copy.wait_recv()

    def more_weights():
        g_down.go()
        g_up.go()

    own_rows = pl.ds(pl.multiple_of(t * 64, 64), 64)
    mixed_b = jnp.concatenate([mixed[0], mixed[1]], axis=1).astype(BF16)
    mix = summed_at_owner(
        mixed_b, out_all, part, paired, sums, relay_a, relay_b, from_left, from_right, more_weights
    )
    value = tokens[0, own_rows, :].astype(F32) + mix
    middle[...] = value
    scale = lax.rsqrt(jnp.mean(value * value, axis=-1, keepdims=True) + EPSILON)
    second[t] = (value * scale * second_gain[...]).astype(BF16)
    to_everyone(lambda b: second.at[b])
    more_weights()

    def raise_rows(i, carry):
        rows = pl.ds(i * 4, 4)
        left = second[rows].reshape(256, 2048)
        for n in range(2):
            cols = slice(n * 256, n * 256 + 256)
            value = jnp.dot(left, up_all[:, :, :, cols].reshape(2048, 256), preferred_element_type=F32)
            value = jnp.maximum(value * rounded(up_scale[:, cols]), 0.0)
            active[pl.ds(pl.multiple_of(i * 256, 256), 256), cols] = (value * value).astype(BF16)
        return carry

    lax.fori_loop(0, 2, raise_rows, 0)
    down = summed_at_owner(
        active[...], down_all, part2, paired2, sums2, relay2_a, relay2_b, from_left2, from_right2, lambda: None
    )
    result[t] = (middle[...] + down).astype(BF16)
    to_everyone(lambda b: result.at[b])
    for copy in started:
        copy.wait_send()


def body(
    tokens, first_gain, in_matrix, in_scale, conv_taps, decay_rate, recall_maps, admit_maps,
    out_matrix, out_scale, second_gain, up_matrix, up_scale, down_matrix, down_scale,
):
    row = lambda v: v.reshape(1, -1)
    vmem = pl.BlockSpec(memory_space=pltpu.VMEM)
    ring = [
        pltpu.VMEM((4, 2, 64, 2048), BF16),
        pltpu.VMEM((4, 64, 2048), BF16),
        pltpu.VMEM((4, 64, 2048), BF16),
        pltpu.VMEM((64, 1024), BF16),
        pltpu.VMEM((64, 1024), BF16),
        pltpu.VMEM((64, 2048), BF16),
        pltpu.VMEM((64, 2048), BF16),
    ]
    out = pl.pallas_call(
        kernel,
        out_shape=jax.ShapeDtypeStruct((8, 64, 2048), BF16),
        in_specs=[vmem] * 15,
        out_specs=vmem,
        scratch_shapes=[
            pltpu.VMEM((NZ, NY, 64, 256), BF16),
            pltpu.VMEM((NZ, NY, 64, 256), BF16),
            pltpu.VMEM((NZ, NY, 64, 512), BF16),
            pltpu.VMEM((NZ, NY, 64, 512), BF16),
            pltpu.VMEM((512, 2048), BF16),
            pltpu.VMEM((2, 512 + 2 * PAD, 128), F32),
            pltpu.VMEM((512, 256), F32),
            pltpu.VMEM((2, 512, 256), F32),
            pltpu.VMEM((2, 512, 256), F32),
            pltpu.VMEM((2, 512, 256), F32),
            pltpu.VMEM((2, 512, 256), F32),
            pltpu.VMEM((2, 512, 128), F32),
            *ring,
            pltpu.VMEM((64, 2048), F32),
            pltpu.VMEM((8, 64, 2048), BF16),
            pltpu.VMEM((512, 512), BF16),
            *ring,
            pltpu.SemaphoreType.DMA((COPIES,)),
            pltpu.SemaphoreType.DMA((COPIES,)),
        ],
        compiler_params=pltpu.CompilerParams(
            collective_id=0, has_side_effects=True, vmem_limit_bytes=60 * 1024 * 1024
        ),
        name="layer",
    )(
        tokens, row(first_gain), in_matrix, row(in_scale), conv_taps, decay_rate, recall_maps, admit_maps,
        out_matrix, row(out_scale), row(second_gain), up_matrix, row(up_scale), down_matrix, row(down_scale),
    )
    return out.reshape(tokens.shape)


def solution(mesh):
    placed = (
        P(("rep", "fs"), None, None),
        P(),
        P("fs", "tp"),
        P("tp"),
        P(None, "tp"),
        P(None, "tp"),
        P(None, "tp", None, None),
        P(None, "tp", None, None),
        P("fs", "tp"),
        P("fs"),
        P(),
        P("fs", "tp"),
        P("tp"),
        P("fs", "tp"),
        P("fs"),
    )
    return jax.shard_map(
        body, mesh=mesh, in_specs=placed, out_specs=P(("rep", "fs"), None, None), check_vma=False
    )
```

time: 506 us -> 134 us (0.26)
  waiting for transfers between devices: 186 us -> 0 us
  Pallas kernels: 0 us -> 130 us
  local copies, waits for them, and re-layouts: 129 us -> 3.16 us
  other arithmetic: 61.6 us -> 0 us
  blocking collectives: 60.3 us -> 0 us
  starting transfers between devices: 32.1 us -> 0 us
  matrix products: 17.1 us -> 0 us
  between operations: 14.1 us -> 0.01 us
    all_gather x2 -> x0, waiting for transfers between devices: 138 us -> none  [the longest x1 138 us: sent_together(): out = lax.all_gather(both, axis, axis=dim, tiled=True)]
    pallas_call x0 -> x1, Pallas kernels: none -> 130 us  [body(): pl.pallas_call(kernel, out_shape=jax.ShapeDtypeStruct((8, 64, 2048), BF16...]
    slice x109 -> x0, local copies, waits for them, and re-layouts: 113 us -> none  [the longest x108 112 us: one_direction(): carried = lax.associative_scan(combine_steps, (decay, drive), axis=0)]
    all_to_all x2 -> x0, blocking collectives: 60.3 us -> none  [the longest x1 30.6 us: sum_at_owner(): lax.all_to_all(pieces, axis, split_axis=0, concat_axis=0, tiled=True)]
    all_to_all x2 -> x0, waiting for transfers between devices: 48.3 us -> none  [the longest x1 26.3 us: from_everyone(): return lax.all_to_all(copies, axis, split_axis=0, concat_axis=0, tiled=True)]
    all_to_all x2 -> x0, starting transfers between devices: 32.1 us -> none  [the longest x1 26.7 us: sum_at_owner(): lax.all_to_all(pieces, axis, split_axis=0, concat_axis=0, tiled=True)]
    mul x15 -> x0, other arithmetic: 18.7 us -> none  [the longest x14 18.1 us: combine_steps(): return (earlier[0] * later[0], later[0] * earlier[1] + later[1])]
    dot_general x7 -> x0, matrix products: 17.1 us -> none  [the longest x2 9.98 us: contract_last(): lax.dot_general(left, right, (((1,), (1,)), ((), ())), preferred_element_...]
  transfers between devices with their start and end apart: 4 -> 0, of which waited for: 3 -> 0; matrix products, arithmetic and copies ran while one was open for 39% -> 0% of each run, Pallas kernels for 0% -> 0%
where the time goes in v1:
time: 134 us; the launch traced here: 133 us
  Pallas kernels  130 us (97%)
  local copies, waits for them, and re-layouts  3.16 us (2%)
    pallas_call x1, Pallas kernels, body(): pl.pallas_call(kernel, out_shape=jax.ShapeDtypeStruct((8, 64, 2048), BF16...  130 us
    unnamed x1, local copies, waits for them, and re-layouts  3.16 us

profile of v1, /device:TPU:1, one launch (start us, length us, event | category | flops | bytes accessed | tf_op | source)
XLA Modules:
  0.0 133.1 jit_solution(14234966336653941482)
XLA Ops:
  0.0 129.9 %layer.1 = bf16[8,64,2048]{2,1,0:T(8,128)(2,1)} custom-call(bf16[1,512,2048]{2,1,0:T(8,128)(2,1)} %tokens.1, f32[1,2048]{1,0:T(1,128)} %bitcast.8, f32[64,256]{1,0:T(8,128)} %in_matrix.1, f32[1,256]{1,0:T(1,128)} %bitcast.11, f32[4,256]{1,0:T(4,128)} %conv_taps.1, f32[2,256]{1,0:T(2,128)} %decay_rate.1, f32[2,1,256,256]{3,2,1,0:T(8,128)} %recall_maps.1, ...), custom_call_target="tpu_custom_call" | custom-call | tf_op jit(solution)/shard_map/layer/pallas_call | solution.py:332
  129.9 3.2 %copy.17 = bf16[1,512,2048]{2,1,0:T(8,128)(2,1)} copy(bf16[1,512,2048]{2,1,0:T(8,128)(2,1)} %bitcast.7) | data formatting | bytes 4194304
